TPU v7x, 128 devices: a whole 4x4x4 slice. The times are simulated.
128 devices in a mesh: fs: 16 (over z, x), tp: 8 (over y, core).
Axes of the slice: x: 4, y: 4, z: 4, core: 2. Of those that a mesh axis runs over, the one named last changes fastest.
Arguments:
- h_saved: bfloat16 [32768, 2048], P('fs'), may hold values from -6 to 6
- conv_cotan: bfloat16 [32768, 2560], P('fs', 'tp'), may hold values from -64 to 64
- lru_out: bfloat16 [32768, 2560], P('fs', 'tp'), may hold values from -64 to 64
- out_cotan: bfloat16 [32768, 2048], P('fs'), may hold values from -6 to 6
- basis_in: bfloat16 [2048, 256], P('fs'), may hold values from -1.41421356 to 1.41421356
- basis_out: bfloat16 [2048, 256], P('fs'), may hold values from -1.41421356 to 1.41421356
- weight_in: float32 [2048, 2560], P('fs', 'tp'), may hold values from -0.125 to 0.125
- weight_out: float32 [2560, 2048], P('tp', 'fs'), may hold values from -0.125 to 0.125
- first_in: float32 [256, 2560], P('fs', 'tp'), may hold values from -6 to 6
- second_in: float32 [256, 2560], P('fs', 'tp'), may hold values from 0.05 to 2
- first_out: float32 [256, 2560], P('fs', 'tp'), may hold values from -6 to 6
- second_out: float32 [256, 2560], P('fs', 'tp'), may hold values from 0.05 to 2
Outputs:
- step_in: float32 [2048, 2560], P('fs', 'tp')
- new_weight_in: float32 [2048, 2560], P('fs', 'tp')
- copy_in: bfloat16 [2048, 2560], P(None, 'tp')
- new_first_in: float32 [256, 2560], P('fs', 'tp')
- new_second_in: float32 [256, 2560], P('fs', 'tp')
- step_out: float32 [2560, 2048], P('tp', 'fs')
- new_weight_out: float32 [2560, 2048], P('tp', 'fs')
- copy_out: bfloat16 [2560, 2048], P('tp')
- new_first_out: float32 [256, 2560], P('fs', 'tp')
- new_second_out: float32 [256, 2560], P('fs', 'tp')
All inputs are finite; a program needn't handle non-finite values.
Results may differ from a plain program's by a relative error of at most 0.0046.
Values may be sent and summed in bfloat16 or wider, within the bound.
No kernel may reach another device: no remote copies, remote signals or barrier semaphores. Data moves between devices by JAX's collectives and lax.ppermute only.
A program may use at most 128 MiB of HBM per device.

v0:
```python
import math
import jax
import jax.numpy as jnp
from jax import lax
from jax.sharding import Mesh
from jax.sharding import PartitionSpec as P

D_RNN = 2560
RANK = 256
FS = ("fs_0", "fs_1")
FS_TP = ("fs_0", "fs_1", "tp_0", "tp_1")
TP = ("tp_0", "tp_1")


def laid_out(blocks, dim):
    blocks = jnp.moveaxis(blocks, 0, dim)
    lengths = blocks.shape
    return blocks.reshape(*lengths[:dim], lengths[dim] * lengths[dim + 1], *lengths[dim + 2 :])


def sent_to_all(array, axis):
    copies = jnp.broadcast_to(array, (lax.axis_size(axis), *array.shape))
    return lax.all_to_all(copies, axis, split_axis=0, concat_axis=0, tiled=True)


def gather_directly(array, axis, dim):
    return laid_out(sent_to_all(array, axis), dim)


def in_one_piece(arrays, axis, dim, along):
    ends, at = ([], 0)
    for a in arrays[:-1]:
        at += a.shape[along]
        ends.append(at)
    both = jnp.concatenate(arrays, axis=along)
    return tuple(jnp.split(gather_directly(both, axis, dim), ends, axis=along))


def split_up(array, dim, size):
    lengths = array.shape
    blocks = array.reshape(*lengths[:dim], size, lengths[dim] // size, *lengths[dim + 1 :])
    return jnp.moveaxis(blocks, dim, 0)


def sent_and_summed(array, axis, dim):
    blocks = split_up(array, dim, lax.axis_size(axis))
    arrived = lax.all_to_all(blocks, axis, split_axis=0, concat_axis=0, tiled=True)
    return arrived.sum(axis=0)


def sent_together(arrays, axis, dim, along):
    both = jnp.concatenate(arrays, axis=along)
    filled, at, done = (sent_and_summed(both, axis, dim), 0, [])
    for a in arrays:
        done.append(lax.slice_in_dim(filled, at, at + a.shape[along], axis=along))
        at += a.shape[along]
    return tuple(done)


def by_axis(array, axes):
    for axis in axes:
        array = lax.psum(array, axis)
    return array


def in_one_piece_2(arrays, axis, dim, along):
    widths = [a.shape[along] for a in arrays]
    both = jnp.concatenate(arrays, axis=along)
    filled = lax.all_gather(both, axis, axis=dim, tiled=True)
    return tuple(jnp.split(filled, [sum(widths[:k]) for k in range(1, len(widths))], axis=along))


def turned_gather(arrays, axis, dims):
    turned = [jnp.moveaxis(a, dim, 0) for a, dim in zip(arrays, dims)]
    widths = [t[0].size for t in turned]
    both = jnp.concatenate([t.reshape(-1, w) for t, w in zip(turned, widths)], axis=1)
    filled = lax.all_gather(both, axis, axis=0, tiled=True)
    blocks = jnp.split(filled, [sum(widths[:k]) for k in range(1, len(widths))], axis=1)
    return tuple(
        (
            jnp.moveaxis(b.reshape(-1, *t.shape[1:]), 0, dim)
            for b, t, dim in zip(blocks, turned, dims)
        )
    )


def split_product(narrow, wide):
    upper = lax.optimization_barrier(wide.astype(jnp.bfloat16))
    lower = (wide - upper.astype(jnp.float32)).astype(jnp.bfloat16)
    turned = jnp.transpose(narrow)
    first_part = jnp.dot(turned, upper, preferred_element_type=jnp.float32)
    second_part = jnp.dot(turned, lower, preferred_element_type=jnp.float32)
    return first_part + second_part


def moments(proj, factor, first, second):
    scaled = factor * proj
    first_new = 0.8 * first + 0.2 * scaled
    second_new = 0.9 * second + 0.1 * scaled * scaled
    direction = (first_new / (jnp.sqrt(second_new) + 1e-08)).astype(jnp.bfloat16)
    return (first_new, second_new, direction)


def shards(
    h_saved,
    conv_cotan,
    lru_out,
    out_cotan,
    basis_in,
    basis_out,
    weight_in,
    weight_out,
    first_in,
    second_in,
    first_out,
    second_out,
):
    pairs = ((h_saved, conv_cotan), (out_cotan, lru_out))
    partial_value = []
    wholes = in_one_piece((basis_in, basis_out), FS, 0, 1)
    for number in range(2):
        reduced = jnp.dot(pairs[number][0], wholes[number], preferred_element_type=jnp.float32)
        partial_value.append(split_product(pairs[number][1], reduced).T)
    proj_in, proj_out = sent_together((partial_value[0], partial_value[1]), FS, 0, 1)
    total = by_axis(jnp.sum(proj_in * proj_in) + jnp.sum(proj_out * proj_out), FS_TP)
    factor = math.sqrt(2.0 * RANK * D_RNN) * lax.rsqrt(total + 1e-06)
    first_a, second_a, dir_in = moments(proj_in, factor, first_in, second_in)
    first_b, second_b, dir_out = moments(proj_out, factor, first_out, second_out)
    full_in, full_out = in_one_piece_2((dir_in, dir_out), FS, 0, 1)
    step_in = jnp.dot(basis_in, full_in, preferred_element_type=jnp.float32)
    step_out = jnp.dot(basis_out, full_out, preferred_element_type=jnp.float32).T
    new_in = weight_in - 0.02 * step_in
    new_out = weight_out - 0.02 * step_out
    copy_in, copy_out = turned_gather(
        (new_in.astype(jnp.bfloat16), new_out.astype(jnp.bfloat16)), FS, (0, 1)
    )
    return (
        step_in,
        new_in,
        copy_in,
        first_a,
        second_a,
        step_out,
        new_out,
        copy_out,
        first_b,
        second_b,
    )


def solution(mesh):
    finer = Mesh(mesh.devices.reshape(4, 4, 4, 2), ("fs_0", "fs_1", "tp_0", "tp_1"))
    placed = (
        P(FS, None),
        P(FS, TP),
        P(FS, TP),
        P(FS, None),
        P(FS, None),
        P(FS, None),
        P(FS, TP),
        P(TP, FS),
        P(FS, TP),
        P(FS, TP),
        P(FS, TP),
        P(FS, TP),
    )
    return jax.shard_map(
        shards,
        mesh=finer,
        in_specs=placed,
        out_specs=(
            P(FS, TP),
            P(FS, TP),
            P(None, TP),
            P(FS, TP),
            P(FS, TP),
            P(TP, FS),
            P(TP, FS),
            P(TP, None),
            P(FS, TP),
            P(FS, TP),
        ),
        check_vma=False,
    )
```

profile of v0, /device:TPU:0, one launch (start us, length us, event | category | flops | bytes accessed | tf_op | source)
XLA Modules:
  0.0 189.7 jit_solution(8411399123699626168)
XLA Ops:
  7.2 1.0 pad_maximum_fusion.2
  8.4 36.4 %all_to_all.10 = bf16[16,128,512]{2,1,0:T(8,128)(2,1)S(1)} all-to-all(bf16[16,128,512]{2,1,0:T(8,128)(2,1)S(1)} %broadcast_in_dim.3), channel_id=1, replica_groups=mesh['fs_0'=4,'fs_1'=4,'tp_0'=4,'tp_1'=2] {'fs_0','fs_1'}, dimensions={0} | all-to-all | bytes 4194304 | tf_op jit(solution)/shard_map/all_to_all | solution.py:23
  44.9 5.9 %fusion.10 = (bf16[2048,256]{0,1:T(8,128)(2,1)S(1)}, f32[2048,256]{0,1:T(8,128)S(1)}) fusion(bf16[2048,2048]{1,0:T(8,128)(2,1)} %param.15, bf16[2048,512]{1,0:T(8,128)(2,1)S(1)} %bitcast.23), kind=kOutput, calls=%fused_computation.33 | convolution fusion | flops 2148007936 | bytes 12582912 | tf_op jit(solution)/shard_map/dot_general | solution.py:122
  50.8 2.4 %fusion.11 = (bf16[2048,256]{0,1:T(8,128)(2,1)S(1)}, f32[2048,256]{0,1:T(8,128)S(1)}) fusion(bf16[2048,2048]{1,0:T(8,128)(2,1)S(1)} %bitcast.26, bf16[2048,512]{1,0:T(8,128)(2,1)S(1)} %bitcast.24), kind=kOutput, calls=%fused_computation.34 | convolution fusion | flops 2148007936 | bytes 12582912 | tf_op jit(solution)/shard_map/dot_general | solution.py:122
  53.2 0.5 fusion.13
  53.8 0.6 convolution_add_fusion
  54.4 0.7 copy-done.1
  55.1 0.5 fusion.12
  55.6 0.6 convolution_add_fusion.1
  56.4 0.2 copy.22
  56.6 15.2 %all_to_all.11 = f32[16,16,640]{2,1,0:T(8,128)S(1)} all-to-all(f32[16,16,640]{2,1,0:T(8,128)S(1)} %bitcast.22), channel_id=1, replica_groups=mesh['fs_0'=4,'fs_1'=4,'tp_0'=4,'tp_1'=2] {'fs_0','fs_1'}, dimensions={0} | all-to-all | bytes 1310720 | tf_op jit(solution)/shard_map/all_to_all | solution.py:47
  71.9 0.7 multiply_reduce_fusion
  73.9 9.1 %psum.28 = f32[]{:T(128)} all-reduce(f32[]{:T(128)S(6)} %add.42), channel_id=1, replica_groups=mesh['fs_0'=4,'fs_1'=4,'tp_0'=4,'tp_1'=2] {'fs_0'}, use_global_device_ids=true, to_apply=%region_3.0 | all-reduce | flops 1 | bytes 8 | tf_op jit(solution)/shard_map/psum | solution.py:62
  83.0 9.6 %psum.29 = f32[]{:T(128)} all-reduce(f32[]{:T(128)} %psum.28), channel_id=1, replica_groups=mesh['fs_0'=4,'fs_1'=4,'tp_0'=4,'tp_1'=2] {'fs_1'}, use_global_device_ids=true, to_apply=%region_4.0 | all-reduce | flops 1 | bytes 8 | tf_op jit(solution)/shard_map/psum | solution.py:62
  92.6 11.4 %psum.30 = f32[]{:T(128)} all-reduce(f32[]{:T(128)} %psum.29), channel_id=1, replica_groups=mesh['fs_0'=4,'fs_1'=4,'tp_0'=4,'tp_1'=2] {'tp_0'}, use_global_device_ids=true, to_apply=%region_5.0 | all-reduce | flops 1 | bytes 8 | tf_op jit(solution)/shard_map/psum | solution.py:62
  103.9 3.1 %psum.31 = f32[]{:T(128)} all-reduce(f32[]{:T(128)} %psum.30), channel_id=1, replica_groups=mesh['fs_0'=4,'fs_1'=4,'tp_0'=4,'tp_1'=2] {'tp_1'}, use_global_device_ids=true, to_apply=%region_6.0 | all-reduce | flops 1 | bytes 8 | tf_op jit(solution)/shard_map/psum | solution.py:62
  107.8 0.7 divide_convert_fusion.1
  108.5 21.7 %all_gather.6 = bf16[256,640]{1,0:T(8,128)(2,1)S(1)} all-gather(bf16[16,640]{1,0:T(8,128)(2,1)S(1)} %pad_maximum_fusion.3), channel_id=1, replica_groups=mesh['fs_0'=4,'fs_1'=4,'tp_0'=4,'tp_1'=2] {'fs_0','fs_1'}, dimensions={0}, use_global_device_ids=true | all-gather | bytes 348160 | tf_op jit(solution)/shard_map/all_gather | solution.py:69
  130.2 0.3 fusion.2
  130.6 1.0 fusion.7
  131.5 0.7 convert_bitcast_fusion
  132.2 0.7 pad_maximum_fusion.1
  132.9 46.4 %all-gather.2.cloned.1.call-done = bf16[2048,640]{0,1:T(8,128)(2,1)} async-done(((bf16[128,640]{0,1:T(8,128)(2,1)}), bf16[2048,640]{0,1:T(8,128)(2,1)}) %all-gather.2.cloned.1.call-update) | async-done | bytes 2621456 | tf_op jit(solution)/shard_map/all_gather | solution.py:77
  179.4 3.5 %slice_bitcast_fusion = (bf16[320,2048]{1,0:T(8,128)(2,1)}, bf16[2048,320]{0,1:T(8,128)(2,1)}) fusion(bf16[2048,640]{0,1:T(8,128)(2,1)} %all-gather.2.cloned.1.call-done), kind=kLoop, calls=%fused_computation.4 | loop fusion | bytes 5242880 | tf_op jit(solution)/shard_map/transpose | solution.py:81
  (32 shorter events, 0.5 us)
Async XLA Ops:
  7.2 46.1 %copy-start = (bf16[2048,320]{0,1:T(8,128)(2,1)S(1)}, bf16[2048,320]{0,1:T(8,128)(2,1)}, u32[]{:S(2)}) copy-start(bf16[2048,320]{0,1:T(8,128)(2,1)} %param.14) | copy-start | bytes 3932164
  7.2 172.2 %all-gather.2.cloned.1.call-start = ((), (), s32[]{:S(2)}) async-start(), calls=%async_computation.2 | async-start | bytes 2785280 | tf_op jit(solution)/shard_map/all_gather | solution.py:77
  8.4 42.4 %slice-start = ((s8[8388608]{0:T(1024)(128)(4,1)}), s8[4194304]{0:T(1024)(128)(4,1)S(1)}, s32[]{:S(2)}) async-start(s8[8388608]{0:T(1024)(128)(4,1)} %bitcast.25), calls=%async_computation.3 | async-start | bytes 8388608
  44.9 5.9 %slice-start.1 = ((s8[8388608]{0:T(1024)(128)(4,1)}), s8[4194304]{0:T(1024)(128)(4,1)S(1)}, s32[]{:S(2)}) async-start(s8[8388608]{0:T(1024)(128)(4,1)} %bitcast.25), calls=%async_computation.4 | async-start | bytes 8388608
  53.8 1.3 copy-start.1
  56.2 51.5 %copy-start.7 = (f32[16,320]{1,0:T(8,128)S(1)}, f32[16,320]{1,0:T(8,128)}, u32[]{:S(2)}) copy-start(f32[16,320]{1,0:T(8,128)} %param.21) | copy-start | bytes 61444
  56.2 51.5 %copy-start.8 = (f32[16,320]{1,0:T(8,128)S(1)}, f32[16,320]{1,0:T(8,128)}, u32[]{:S(2)}) copy-start(f32[16,320]{1,0:T(8,128)} %param.20) | copy-start | bytes 61444
  56.3 51.5 %copy-start.9 = (f32[16,320]{1,0:T(8,128)S(1)}, f32[16,320]{1,0:T(8,128)}, u32[]{:S(2)}) copy-start(f32[16,320]{1,0:T(8,128)} %param.23) | copy-start | bytes 61444
  56.3 51.5 %copy-start.10 = (f32[16,320]{1,0:T(8,128)S(1)}, f32[16,320]{1,0:T(8,128)}, u32[]{:S(2)}) copy-start(f32[16,320]{1,0:T(8,128)} %param.22) | copy-start | bytes 61444
  56.3 73.9 %copy-start.4 = (bf16[128,256]{1,0:T(8,128)(2,1)S(1)}, bf16[128,256]{1,0:T(8,128)(2,1)}, u32[]{:S(2)}) copy-start(bf16[128,256]{1,0:T(8,128)(2,1)} %param.17) | copy-start | bytes 196612
  56.3 74.2 %copy-start.3 = (bf16[128,256]{1,0:T(8,128)(2,1)S(1)}, bf16[128,256]{1,0:T(8,128)(2,1)}, u32[]{:S(2)}) copy-start(bf16[128,256]{1,0:T(8,128)(2,1)} %param.16) | copy-start | bytes 196612
  56.4 74.2 %copy-start.5 = (f32[128,320]{0,1:T(8,128)S(1)}, f32[128,320]{0,1:T(8,128)}, u32[]{:S(2)}) copy-start(f32[128,320]{0,1:T(8,128)} %param.18) | copy-start | bytes 491524
  56.6 74.9 %copy-start.6 = (f32[320,128]{1,0:T(8,128)S(1)}, f32[320,128]{1,0:T(8,128)}, u32[]{:S(2)}) copy-start(f32[320,128]{1,0:T(8,128)} %param.19) | copy-start | bytes 491524
  130.5 52.4 %copy-start.2 = (f32[320,128]{1,0:T(8,128)}, f32[320,128]{1,0:T(8,128)S(1)}, u32[]{:S(2)}) copy-start(f32[320,128]{1,0:T(8,128)S(1)} %fusion.2) | copy-start | bytes 491524
Sparse Core Ops, SparseCore 0:
  133.0 46.2 all-gather.1
where the time goes:
time: 190 us
  blocking collectives  106 us (56%)
  waiting for transfers between devices  46.5 us (24%)
  between operations  16.3 us (9%)
  matrix products  11.8 us (6%)
  local copies, waits for them, and re-layouts  4.78 us (3%)
  other arithmetic  3.89 us (2%)
    all_gather x1, waiting for transfers between devices, turned_gather(): filled = lax.all_gather(both, axis, axis=0, tiled=True)  46.4 us
    all_to_all x1, blocking collectives, sent_to_all(): return lax.all_to_all(copies, axis, split_axis=0, concat_axis=0, tiled=True)  36.4 us
    psum x4, blocking collectives, by_axis(): array = lax.psum(array, axis)  33.1 us
    all_gather x1, blocking collectives, in_one_piece_2(): filled = lax.all_gather(both, axis, axis=dim, tiled=True)  21.7 us
    all_to_all x1, blocking collectives, sent_and_summed(): lax.all_to_all(blocks, axis, split_axis=0, concat_axis=0, tiled=True)  15.2 us
    dot_general x2, matrix products, shards(): jnp.dot(pairs[number][0], wholes[number], preferred_element_type=jnp.floa...  8.31 us
  transfers between devices with their start and end apart: 1, of which 1 were waited for; matrix products, arithmetic and copies ran while one was open for 0% of the time, Pallas kernels for 0%

commit v1 on v0

--- a/solution.py
+++ b/solution.py
@@ -59,7 +59,12 @@
 
 def by_axis(array, axes):
     for axis in axes:
-        array = lax.psum(array, axis)
+
+        def bench_resolve(target):
+            built = jax.lax.all_gather(target, axis).sum(axis=0)
+            return built
+
+        array = bench_resolve(array)
     return array
 
 

time: 190 us -> 198 us (1.042)
  blocking collectives: 106 us -> 88.7 us
  waiting for transfers between devices: 46.5 us -> 57.4 us
  local copies, waits for them, and re-layouts: 4.78 us -> 13 us
  starting transfers between devices: 0.04 us -> 3.77 us
  other arithmetic: 3.89 us -> 6.32 us
    psum x4 -> x0, blocking collectives: 33.1 us -> none  [by_axis(): array = lax.psum(array, axis)]
    unnamed x0 -> x4, blocking collectives: none -> 30.3 us
    all_to_all x1 -> x0, blocking collectives: 15.2 us -> none  [sent_and_summed(): lax.all_to_all(blocks, axis, split_axis=0, concat_axis=0, tiled=True)]
    all_to_all x0 -> x1, waiting for transfers between devices: none -> 11.2 us  [sent_and_summed(): lax.all_to_all(blocks, axis, split_axis=0, concat_axis=0, tiled=True)]
    unnamed x26 -> x46, local copies, waits for them, and re-layouts: 0.83 us -> 8.16 us
    all_to_all x0 -> x1, starting transfers between devices: none -> 3.73 us  [sent_and_summed(): lax.all_to_all(blocks, axis, split_axis=0, concat_axis=0, tiled=True)]
    reduce_sum x0 -> x4, other arithmetic: none -> 2.41 us  [bench_resolve(): built = jax.lax.all_gather(target, axis).sum(axis=0)]
  transfers between devices with their start and end apart: 1 -> 2, of which waited for: 1 -> 2; matrix products, arithmetic and copies ran while one was open for 0% -> 0% of each run, Pallas kernels for 0% -> 0%
where the time goes in v1:
time: 198 us; the launch traced here: 197 us
  blocking collectives  88.7 us (45%)
  waiting for transfers between devices  57.4 us (29%)
  between operations  16.3 us (8%)
  local copies, waits for them, and re-layouts  13 us (7%)
  matrix products  11.8 us (6%)
  other arithmetic  6.32 us (3%)
  starting transfers between devices  3.77 us (2%)
    all_gather x1, waiting for transfers between devices, turned_gather(): filled = lax.all_gather(both, axis, axis=0, tiled=True)  46.2 us
    all_to_all x1, blocking collectives, sent_to_all(): return lax.all_to_all(copies, axis, split_axis=0, concat_axis=0, tiled=True)  36.4 us
    unnamed x4, blocking collectives  30.3 us
    all_gather x1, blocking collectives, in_one_piece_2(): filled = lax.all_gather(both, axis, axis=dim, tiled=True)  21.9 us
    all_to_all x1, waiting for transfers between devices, sent_and_summed(): lax.all_to_all(blocks, axis, split_axis=0, concat_axis=0, tiled=True)  11.2 us
    dot_general x2, matrix products, shards(): jnp.dot(pairs[number][0], wholes[number], preferred_element_type=jnp.floa...  8.31 us
    unnamed x46, local copies, waits for them, and re-layouts  8.16 us
  transfers between devices with their start and end apart: 2, of which 2 were waited for; matrix products, arithmetic and copies ran while one was open for 0% of the time, Pallas kernels for 0%

profile of v1, /device:TPU:0, one launch (start us, length us, event | category | flops | bytes accessed | tf_op | source)
XLA Modules:
  0.0 197.2 jit_solution(12693672781650655608)
XLA Ops:
  7.2 1.0 pad_maximum_fusion.2
  8.4 36.4 %all_to_all.10 = bf16[16,128,512]{2,1,0:T(8,128)(2,1)S(1)} all-to-all(bf16[16,128,512]{2,1,0:T(8,128)(2,1)S(1)} %broadcast_in_dim.3), channel_id=1, replica_groups=mesh['fs_0'=4,'fs_1'=4,'tp_0'=4,'tp_1'=2] {'fs_0','fs_1'}, dimensions={0} | all-to-all | bytes 4194304 | tf_op jit(solution)/shard_map/all_to_all | solution.py:23
  44.8 5.9 %fusion.10 = (bf16[2048,256]{0,1:T(8,128)(2,1)S(1)}, f32[2048,256]{0,1:T(8,128)S(1)}) fusion(bf16[2048,2048]{1,0:T(8,128)(2,1)} %param.15, bf16[2048,512]{1,0:T(8,128)(2,1)S(1)} %bitcast.30), kind=kOutput, calls=%fused_computation.33 | convolution fusion | flops 2148007936 | bytes 12582912 | tf_op jit(solution)/shard_map/dot_general | solution.py:127
  50.8 2.4 %fusion.11 = (bf16[2048,256]{0,1:T(8,128)(2,1)S(1)}, f32[2048,256]{0,1:T(8,128)S(1)}) fusion(bf16[2048,2048]{1,0:T(8,128)(2,1)S(1)} %bitcast.33, bf16[2048,512]{1,0:T(8,128)(2,1)S(1)} %bitcast.31), kind=kOutput, calls=%fused_computation.34 | convolution fusion | flops 2148007936 | bytes 12582912 | tf_op jit(solution)/shard_map/dot_general | solution.py:127
  54.3 0.7 copy-done.1
  56.4 1.1 copy.22
  57.5 3.7 %all-to-all-start.1 = ((f32[16,16,640]{2,1,0:T(8,128)}), f32[16,16,640]{2,1,0:T(8,128)S(1)}, u32[]{:S(2)}, u32[]{:S(2)}) async-start(f32[16,16,640]{2,1,0:T(8,128)} %bitcast.3), calls=%async_computation.1 | async-start | bytes 1310720 | tf_op jit(solution)/shard_map/all_to_all | solution.py:47
  61.8 11.2 %all-to-all-done.1 = f32[16,16,640]{2,1,0:T(8,128)S(1)} async-done(((f32[16,16,640]{2,1,0:T(8,128)}), f32[16,16,640]{2,1,0:T(8,128)S(1)}, u32[]{:S(2)}, u32[]{:S(2)}) %all-to-all-start.1) | async-done | bytes 655392 | tf_op jit(solution)/shard_map/all_to_all | solution.py:47
  73.1 0.7 multiply_reduce_fusion
  75.1 0.8 dynamic-update-slice
  76.4 8.5 %all-reduce = f32[4]{0:T(128)S(1)} all-reduce(f32[4]{0:T(128)S(1)} %dynamic-update-slice), channel_id=1, replica_groups=mesh['fs_0'=4,'fs_1'=4,'tp_0'=4,'tp_1'=2] {'fs_0'}, use_global_device_ids=true, to_apply=%add | all-reduce | flops 4 | bytes 32
  85.5 1.4 dynamic-update-slice.1
  87.5 8.6 %all-reduce.1 = f32[4]{0:T(128)S(1)} all-reduce(f32[4]{0:T(128)S(1)} %dynamic-update-slice.1), channel_id=1, replica_groups=mesh['fs_0'=4,'fs_1'=4,'tp_0'=4,'tp_1'=2] {'fs_1'}, use_global_device_ids=true, to_apply=%add.1 | all-reduce | flops 4 | bytes 32
  96.7 1.4 dynamic-update-slice.2
  98.7 10.7 %all-reduce.2 = f32[4]{0:T(128)S(1)} all-reduce(f32[4]{0:T(128)S(1)} %dynamic-update-slice.2), channel_id=1, replica_groups=mesh['fs_0'=4,'fs_1'=4,'tp_0'=4,'tp_1'=2] {'tp_0'}, use_global_device_ids=true, to_apply=%add.2 | all-reduce | flops 4 | bytes 32
  110.0 1.4 dynamic-update-slice.3
  111.4 2.4 %all-reduce.3 = f32[2]{0:T(128)S(1)} all-reduce(f32[2]{0:T(128)S(1)} %dynamic-update-slice.3), channel_id=1, replica_groups=mesh['fs_0'=4,'fs_1'=4,'tp_0'=4,'tp_1'=2] {'tp_1'}, use_global_device_ids=true, to_apply=%add.3 | all-reduce | flops 2 | bytes 16
  115.2 0.7 divide_convert_fusion.1
  116.0 21.9 %all_gather.38 = bf16[256,640]{1,0:T(8,128)(2,1)S(1)} all-gather(bf16[16,640]{1,0:T(8,128)(2,1)S(1)} %pad_maximum_fusion.3), channel_id=1, replica_groups=mesh['fs_0'=4,'fs_1'=4,'tp_0'=4,'tp_1'=2] {'fs_0','fs_1'}, dimensions={0}, use_global_device_ids=true | all-gather | bytes 348160 | tf_op jit(solution)/shard_map/all_gather | solution.py:74
  138.3 1.0 fusion.7
  139.3 0.7 convert_bitcast_fusion
  140.0 0.7 pad_maximum_fusion.1
  140.7 46.2 %all-gather.2.cloned.1.call-done = bf16[2048,640]{0,1:T(8,128)(2,1)} async-done(((bf16[128,640]{0,1:T(8,128)(2,1)}), bf16[2048,640]{0,1:T(8,128)(2,1)}) %all-gather.2.cloned.1.call-update) | async-done | bytes 2621456 | tf_op jit(solution)/shard_map/all_gather | solution.py:82
  186.8 3.5 %slice_bitcast_fusion = (bf16[320,2048]{1,0:T(8,128)(2,1)}, bf16[2048,320]{0,1:T(8,128)(2,1)}) fusion(bf16[2048,640]{0,1:T(8,128)(2,1)} %all-gather.2.cloned.1.call-done), kind=kLoop, calls=%fused_computation.4 | loop fusion | bytes 5242880 | tf_op jit(solution)/shard_map/transpose | solution.py:86
  (57 shorter events, 7.8 us)
Async XLA Ops:
  7.2 46.0 %copy-start = (bf16[2048,320]{0,1:T(8,128)(2,1)S(1)}, bf16[2048,320]{0,1:T(8,128)(2,1)}, u32[]{:S(2)}) copy-start(bf16[2048,320]{0,1:T(8,128)(2,1)} %param.14) | copy-start | bytes 3932164
  8.4 42.4 %slice-start = ((s8[8388608]{0:T(1024)(128)(4,1)}), s8[4194304]{0:T(1024)(128)(4,1)S(1)}, s32[]{:S(2)}) async-start(s8[8388608]{0:T(1024)(128)(4,1)} %bitcast.32), calls=%async_computation.3 | async-start | bytes 8388608
  44.8 5.9 %slice-start.1 = ((s8[8388608]{0:T(1024)(128)(4,1)}), s8[4194304]{0:T(1024)(128)(4,1)S(1)}, s32[]{:S(2)}) async-start(s8[8388608]{0:T(1024)(128)(4,1)} %bitcast.32), calls=%async_computation.4 | async-start | bytes 8388608
  53.7 1.3 copy-start.1
  56.2 5.1 %copy-start.14 = (u32[128]{0:T(128)S(1)}, u32[128]{0:T(128)}, u32[]{:S(2)}) copy-start(u32[128]{0:T(128)} %constant.21) | copy-start | bytes 1540
  56.2 19.6 %copy-start.13 = (u32[128]{0:T(128)S(1)}, u32[128]{0:T(128)}, u32[]{:S(2)}) copy-start(u32[128]{0:T(128)} %constant.26) | copy-start | bytes 1540
  56.2 30.7 %copy-start.12 = (u32[128]{0:T(128)S(1)}, u32[128]{0:T(128)}, u32[]{:S(2)}) copy-start(u32[128]{0:T(128)} %constant.31) | copy-start | bytes 1540
  56.2 41.9 %copy-start.11 = (u32[128]{0:T(128)S(1)}, u32[128]{0:T(128)}, u32[]{:S(2)}) copy-start(u32[128]{0:T(128)} %constant.36) | copy-start | bytes 1540
  56.3 58.9 %copy-start.7 = (f32[16,320]{1,0:T(8,128)S(1)}, f32[16,320]{1,0:T(8,128)}, u32[]{:S(2)}) copy-start(f32[16,320]{1,0:T(8,128)} %param.21) | copy-start | bytes 61444
  56.3 58.9 %copy-start.8 = (f32[16,320]{1,0:T(8,128)S(1)}, f32[16,320]{1,0:T(8,128)}, u32[]{:S(2)}) copy-start(f32[16,320]{1,0:T(8,128)} %param.20) | copy-start | bytes 61444
  56.3 58.9 %copy-start.9 = (f32[16,320]{1,0:T(8,128)S(1)}, f32[16,320]{1,0:T(8,128)}, u32[]{:S(2)}) copy-start(f32[16,320]{1,0:T(8,128)} %param.23) | copy-start | bytes 61444
  56.3 58.9 %copy-start.10 = (f32[16,320]{1,0:T(8,128)S(1)}, f32[16,320]{1,0:T(8,128)}, u32[]{:S(2)}) copy-start(f32[16,320]{1,0:T(8,128)} %param.22) | copy-start | bytes 61444
  56.4 81.6 %copy-start.4 = (bf16[128,256]{1,0:T(8,128)(2,1)S(1)}, bf16[128,256]{1,0:T(8,128)(2,1)}, u32[]{:S(2)}) copy-start(bf16[128,256]{1,0:T(8,128)(2,1)} %param.17) | copy-start | bytes 196612
  56.4 81.9 %copy-start.3 = (bf16[128,256]{1,0:T(8,128)(2,1)S(1)}, bf16[128,256]{1,0:T(8,128)(2,1)}, u32[]{:S(2)}) copy-start(bf16[128,256]{1,0:T(8,128)(2,1)} %param.16) | copy-start | bytes 196612
  56.4 81.9 %copy-start.5 = (f32[128,320]{0,1:T(8,128)S(1)}, f32[128,320]{0,1:T(8,128)}, u32[]{:S(2)}) copy-start(f32[128,320]{0,1:T(8,128)} %param.18) | copy-start | bytes 491524
  57.5 81.8 %copy-start.6 = (f32[320,128]{1,0:T(8,128)S(1)}, f32[320,128]{1,0:T(8,128)}, u32[]{:S(2)}) copy-start(f32[320,128]{1,0:T(8,128)} %param.19) | copy-start | bytes 491524
  57.5 15.6 %all-to-all-start.1 = ((f32[16,16,640]{2,1,0:T(8,128)}), f32[16,16,640]{2,1,0:T(8,128)S(1)}, u32[]{:S(2)}, u32[]{:S(2)}) async-start(f32[16,16,640]{2,1,0:T(8,128)} %bitcast.3), calls=%async_computation.1 | async-start | bytes 1310720 | tf_op jit(solution)/shard_map/all_to_all | solution.py:47
  61.2 125.6 %all-gather.2.cloned.1.call-start = ((), (), s32[]{:S(2)}) async-start(), calls=%async_computation.2 | async-start | bytes 2785280 | tf_op jit(solution)/shard_map/all_gather | solution.py:82
  138.3 52.1 %copy-start.2 = (f32[320,128]{1,0:T(8,128)}, f32[320,128]{1,0:T(8,128)S(1)}, u32[]{:S(2)}) copy-start(f32[320,128]{1,0:T(8,128)S(1)} %fusion.2) | copy-start | bytes 491524
Sparse Core Ops, SparseCore 0:
  140.8 46.0 all-gather.1
